TPU v7x, 32 devices: a whole 2x2x4 slice. The times are simulated.
32 devices in a mesh: sp: 16 (over z, y, x), tp: 2 (over core).
Axes of the slice: x: 2, y: 2, z: 4, core: 2. Of those that a mesh axis runs over, the one named last changes fastest.
Arguments:
- hidden_in: bfloat16 [4096, 2048], P('sp'), may hold values from -16 to 16
- query_one: bfloat16 [2048, 512], P(None, 'tp'), may hold values from -0.13258252 to 0.13258252
- query_two: bfloat16 [2048, 512], P(None, 'tp'), may hold values from -0.13258252 to 0.13258252
- key_one: bfloat16 [2048, 512], P(None, 'tp'), may hold values from -0.13258252 to 0.13258252
- key_two: bfloat16 [2048, 512], P(None, 'tp'), may hold values from -0.13258252 to 0.13258252
- value_proj: bfloat16 [2048, 1024], P(None, 'tp'), may hold values from -0.125 to 0.125
- lambdas: float32 [8], P('tp'), may hold values from 0.3 to 0.8
- norm_gain: float32 [128], replicated, may hold values from 0.1 to 1.9
- out_proj: bfloat16 [1024, 2048], P('tp'), may hold values from -0.1875 to 0.1875
Outputs:
- attended: bfloat16 [4096, 2048], P('sp')
All inputs are finite; a program needn't handle non-finite values.
Results may differ from a plain program's by a relative error of at most 0.015.
Values may be sent and summed in bfloat16 or wider, within the bound.
A program may use at most 64 MiB of HBM per device.

v0:
```python
import math
import jax
import jax.numpy as jnp
from jax import lax
from jax.sharding import PartitionSpec as P

epsilon = 1e-06
masked_score = -1e30


def shards(
    hidden_in, query_one, query_two, key_one, key_two, value_proj, lambdas, norm_gain, out_proj
):
    heads_dev = lambdas.shape[0]
    head_qk = query_one.shape[1] // heads_dev
    head_v = value_proj.shape[1] // heads_dev
    width_q = heads_dev * head_qk
    score_scale = 1.75 * head_qk ** (-0.5)
    joined = jnp.concatenate((query_one, query_two, key_one, key_two, value_proj), axis=1)
    projected = jnp.dot(hidden_in, joined, preferred_element_type=jnp.float32).astype(jnp.bfloat16)
    tok_rows = projected.shape[0]
    key_values = projected[:, 2 * width_q :]
    my_index = lax.axis_index("sp")
    offset = my_index * tok_rows
    query_sets = (projected[:, : 2 * width_q],)
    position_sets = (offset + jnp.arange(tok_rows, dtype=jnp.int32),)
    groups = []
    for query_rows, positions in zip(query_sets, position_sets):
        group_rows = query_rows.shape[0]
        query_a = query_rows[:, :width_q].reshape(group_rows, heads_dev, head_qk)
        query_b = query_rows[:, width_q:].reshape(group_rows, heads_dev, head_qk)
        groups.append((query_a, query_b, positions, positions[group_rows - 1]))

    def one_map(queries, keys, value_rows, allowed, running_max, running_sum, accum):
        scores = (
            jnp.einsum("qhd,khd->hqk", queries, keys, preferred_element_type=jnp.float32)
            * score_scale
        )
        scores = jnp.where(allowed[None], scores, masked_score)
        new_max = jnp.maximum(running_max, jnp.max(scores, axis=-1))
        rescale = jnp.exp(running_max - new_max)
        weights = jnp.where(allowed[None], jnp.exp(scores - new_max[..., None]), 0.0)
        new_sum = running_sum * rescale + jnp.sum(weights, axis=-1)
        added = jnp.einsum(
            "hqk,khe->hqe",
            weights.astype(jnp.bfloat16),
            value_rows,
            preferred_element_type=jnp.float32,
        )
        return (new_max, new_sum, accum * rescale[..., None] + added)

    def absorb(group_state, group, kblock, kstart):
        query_a, query_b, positions, last_pos = group
        block_rows = kblock.shape[0]
        k_pos = kstart + jnp.arange(block_rows, dtype=jnp.int32)
        allowed = k_pos[None, :] <= positions[:, None]
        keys_a = kblock[:, :width_q].reshape(block_rows, heads_dev, head_qk)
        keys_b = kblock[:, width_q : 2 * width_q].reshape(block_rows, heads_dev, head_qk)
        value_rows = kblock[:, 2 * width_q :].reshape(block_rows, heads_dev, head_v)
        first_map = one_map(query_a, keys_a, value_rows, allowed, *group_state[:3])
        second_map = one_map(query_b, keys_b, value_rows, allowed, *group_state[3:])
        return first_map + second_map

    group = groups[0]
    group_rows = group[0].shape[0]
    start_max = jnp.full((heads_dev, group_rows), masked_score, jnp.float32)
    start_sum = jnp.zeros((heads_dev, group_rows), jnp.float32)
    start_acc = jnp.zeros((heads_dev, group_rows, head_v), jnp.float32)
    initial_list = [(start_max, start_sum, start_acc, start_max, start_sum, start_acc)]
    initial = tuple(initial_list)
    softmax_state = initial
    kv_piece = lax.all_gather(key_values, "sp", axis=0, tiled=True)
    piece_rows = kv_piece.shape[0]
    block_rows = math.gcd(piece_rows, 512)
    block_count = piece_rows // block_rows
    stacked = kv_piece.reshape(block_count, block_rows, kv_piece.shape[1])

    def absorb_step(carried, blocks_in):
        kblock, block_index = blocks_in
        kstart = block_index * block_rows
        renewed = []
        for group, group_state in zip(groups, carried):
            renewed.append(
                lax.cond(
                    kstart <= group[3],
                    lambda inner, group=group: absorb(inner, group, kblock, kstart),
                    lambda inner: inner,
                    group_state,
                )
            )
        return (tuple(renewed), None)

    softmax_state, _ = lax.scan(
        absorb_step, softmax_state, (stacked, jnp.arange(block_count, dtype=jnp.int32))
    )
    normed_sets = []
    for group_state in softmax_state:
        out_a = group_state[2] / group_state[1][..., None]
        out_b = group_state[5] / group_state[4][..., None]
        mixed_out = out_a - lambdas[:, None, None] * out_b
        scale_rows = lax.rsqrt(jnp.mean(mixed_out * mixed_out, axis=-1, keepdims=True) + epsilon)
        normed = (mixed_out * scale_rows * norm_gain).astype(jnp.bfloat16)
        group_rows = normed.shape[1]
        normed_sets.append(jnp.transpose(normed, (1, 0, 2)).reshape(group_rows, heads_dev * head_v))
    normed_all = normed_sets[0]
    partial_value = jnp.dot(normed_all, out_proj, preferred_element_type=jnp.float32)
    result = lax.psum(partial_value.astype(jnp.bfloat16), "tp")
    return result


def solution(mesh):
    placed = (
        P("sp", None),
        P(None, "tp"),
        P(None, "tp"),
        P(None, "tp"),
        P(None, "tp"),
        P(None, "tp"),
        P("tp"),
        P(),
        P("tp", None),
    )
    return jax.shard_map(
        shards, mesh=mesh, in_specs=placed, out_specs=P("sp", None), check_vma=False
    )
```

profile of v0, /device:TPU:0, one launch (start us, length us, event | category | flops | bytes accessed | tf_op | source)
XLA Modules:
  0.0 254.4 jit_solution(17439998530829736582)
XLA Ops:
  6.5 0.0 copy-start
  6.5 0.0 all-gather.2.cloned.1.call-start
  6.5 1.5 constant_dynamic-update-slice_fusion.4
  8.0 0.2 copy-done.2
  8.2 0.1 constant_dynamic-update-slice_fusion.3
  8.3 0.2 copy-done.3
  8.5 0.1 constant_dynamic-update-slice_fusion.2
  8.6 0.9 copy-done.4
  9.5 0.1 constant_dynamic-update-slice_fusion.1
  9.6 0.6 copy-done.1
  10.2 0.1 constant_dynamic-update-slice_fusion
  10.3 1.1 copy-done.7
  11.4 1.8 fusion.24
  13.3 0.8 slice.34
  14.1 0.0 all-gather.2.cloned.1.call-update
  14.1 0.0 all-reduce.2.cloned.1.call-start
  14.2 0.7 slice.27
  14.9 136.6 %all-gather.2.cloned.1.call-done = bf16[4096,1024]{0,1:T(8,128)(2,1)} async-done(((bf16[256,1024]{0,1:T(8,128)(2,1)}), bf16[4096,1024]{0,1:T(8,128)(2,1)}) %all-gather.2.cloned.1.call-update) | async-done | bytes 8388624 | tf_op jit(solution)/shard_map/all_gather | solution.py:72
  151.5 7.4 %copy.26 = bf16[128,8,8,512]{3,2,0,1:T(8,128)(2,1)} copy(bf16[128,8,8,512]{3,2,1,0:T(8,128)(2,1)} %bitcast.57) | data formatting | bytes 16777216 | tf_op jit(solution)/shard_map/reshape | solution.py:76
  159.0 21.9 %while.21 = (s32[]{:T(128)}, f32[4,256]{1,0:T(4,128)S(1)}, f32[4,256]{1,0:T(4,128)S(1)}, f32[4,256,128]{2,1,0:T(8,128)S(1)}, f32[4,256]{1,0:T(4,128)S(1)}, /*ind...) while((s32[]{:T(128)}, f32[4,256]{1,0:T(4,128)S(1)}, ...), condition=%wide.region_7.8_spmd.clone, body=%wide.region_0.7_spmd.clone.sunk | while | flops 416944896 | bytes 23601552 | solution.py:93
  159.1 0.6 dynamic_slice.13
  161.0 6.1 %conditional.3 = ((f32[4,256]{1,0:T(4,128)S(1)}, f32[4,256]{1,0:T(4,128)S(1)}, f32[4,256,128]{2,1,0:T(8,128)S(1)}, f32[4,256]{1,0:T(4,128)S(1)}, f32[4,256]{1,0:T(4,128)S(1)}, /*index=5*/f32[4,256,128]{2,1,0:T(8,128)S(1)})) conditional(s32[]{:T(128)} %convert_element_type.38, (f32[4,256]{1,0:T(4,128)S(1)}, f32[4,256]{1,0:T(4,128)S(1)}, ...), branch_computations={%region_1.1_spmd, %region_2.6_spmd} | conditional | flops 416944896 | bytes 23600196 | solution.py:84
  161.0 1.3 dynamic-slice_bitcast_fusion
  162.4 0.5 fusion.27
  162.9 0.1 broadcast_compare_fusion
  163.0 0.7 fusion.3
  163.8 1.0 fusion.7
  164.9 1.1 convolution_add_fusion
  165.9 1.1 convolution_add_fusion.1
  167.1 0.6 dynamic_slice.13
  169.1 0.6 dynamic_slice.13
  171.0 0.6 dynamic_slice.13
  173.0 0.6 dynamic_slice.13
  175.0 0.6 dynamic_slice.13
  177.0 0.6 dynamic_slice.13
  179.0 0.6 dynamic_slice.13
  180.9 0.0 copy-start.5
  180.9 0.0 copy-start.6
  180.9 1.0 copy.18
  181.9 0.2 copy.19
  182.2 1.2 multiply_reduce_fusion
  183.4 0.0 copy-done.6
  183.4 0.1 multiply_convert_fusion
  183.5 0.0 copy-done
  183.5 1.7 convolution_convert_fusion
  185.2 0.0 all-reduce.2.cloned.1.call-update
  185.2 60.0 %all-reduce.2.cloned.1.call-done = bf16[256,2048]{1,0:T(8,128)(2,1)} async-done(((bf16[256,2048]{1,0:T(8,128)(2,1)}), bf16[256,2048]{1,0:T(8,128)(2,1)}) %all-reduce.2.cloned.1.call-update) | async-done | bytes 1048592 | tf_op jit(solution)/shard_map/psum | solution.py:107
  245.3 2.3 copy.67
  (40 shorter events, 0.4 us)
Async XLA Ops:
  6.5 177.0 %copy-start = (bf16[512,2048]{1,0:T(8,128)(2,1)S(1)}, bf16[512,2048]{1,0:T(8,128)(2,1)}, u32[]{:S(2)}) copy-start(bf16[512,2048]{1,0:T(8,128)(2,1)} %param.21) | copy-start | bytes 6291460
  6.5 1.7 copy-start.2
  6.5 145.0 %all-gather.2.cloned.1.call-start = ((), (), s32[]{:S(2)}) async-start(), calls=%async_computation | async-start | bytes 8912896 | tf_op jit(solution)/shard_map/all_gather | solution.py:72
  6.5 2.0 copy-start.3
  8.2 1.3 copy-start.4
  8.5 1.7 copy-start.1
  10.2 1.2 copy-start.7
  14.1 231.1 %all-reduce.2.cloned.1.call-start = ((), (), s32[]{:S(2)}) async-start(), calls=%async_computation.1 | async-start | bytes 2097152 | tf_op jit(solution)/shard_map/psum | solution.py:107
  180.9 1.2 copy-start.5
  180.9 2.4 copy-start.6
Sparse Core Ops, SparseCore 0:
  14.3 137.1 all-gather.1
  185.3 59.8 all-reduce.1
where the time goes:
time: 255 us; the launch traced here: 254 us
  waiting for transfers between devices  197 us (77%)
  local copies, waits for them, and re-layouts  23.5 us (9%)
  between operations  13.6 us (5%)
  loops' own time  11.2 us (4%)
  matrix products  6.91 us (3%)
    all_gather x1, waiting for transfers between devices, shards(): kv_piece = lax.all_gather(key_values, 'sp', axis=0, tiled=True)  137 us
    psum x1, waiting for transfers between devices, shards(): result = lax.psum(partial_value.astype(jnp.bfloat16), 'tp')  60 us
    another operation x1, loops' own time, shards(): lax.scan(absorb_step, softmax_state, (stacked, jnp.arange(block_count, dt...  11 us
    reshape x1, local copies, waits for them, and re-layouts, shards(): stacked = kv_piece.reshape(block_count, block_rows, kv_piece.shape[1])  7.41 us
    unnamed x21, local copies, waits for them, and re-layouts  7.03 us
  transfers between devices with their start and end apart: 2, of which 2 were waited for; matrix products, arithmetic and copies ran while one was open for 0% of the time, Pallas kernels for 0%

commit v1 on v0

--- a/solution.py
+++ b/solution.py
@@ -3,9 +3,16 @@
 import jax.numpy as jnp
 from jax import lax
 from jax.sharding import PartitionSpec as P
+from jax.lax import all_gather
 
 epsilon = 1e-06
 masked_score = -1e30
+
+
+def proceed_stacks_all(page, shard_axis):
+    extra = all_gather(page, shard_axis)
+    block_next = jnp.sum(extra, 0)
+    return block_next
 
 
 def shards(
@@ -104,7 +111,7 @@
         normed_sets.append(jnp.transpose(normed, (1, 0, 2)).reshape(group_rows, heads_dev * head_v))
     normed_all = normed_sets[0]
     partial_value = jnp.dot(normed_all, out_proj, preferred_element_type=jnp.float32)
-    result = lax.psum(partial_value.astype(jnp.bfloat16), "tp")
+    result = proceed_stacks_all(partial_value.astype(jnp.bfloat16), "tp")
     return result
 
 

time: 255 us -> 247 us (0.969)
  waiting for transfers between devices: 197 us -> 188 us
  other arithmetic: 2.53 us -> 5.82 us
    psum x1 -> x0, waiting for transfers between devices: 60 us -> none  [shards(): result = lax.psum(partial_value.astype(jnp.bfloat16), 'tp')]
    all_gather x0 -> x1, waiting for transfers between devices: none -> 51.3 us  [proceed_stacks_all(): extra = all_gather(page, shard_axis)]
    reduce_sum x0 -> x1, other arithmetic: none -> 3.31 us  [proceed_stacks_all(): block_next = jnp.sum(extra, 0)]
    unnamed x21 -> x20, local copies, waits for them, and re-layouts: 7.03 us -> 4.73 us
where the time goes in v1:
time: 247 us
  waiting for transfers between devices  188 us (76%)
  local copies, waits for them, and re-layouts  21.1 us (9%)
  between operations  13.6 us (6%)
  loops' own time  11.2 us (5%)
  matrix products  6.94 us (3%)
  other arithmetic  5.82 us (2%)
    all_gather x1, waiting for transfers between devices, shards(): kv_piece = lax.all_gather(key_values, 'sp', axis=0, tiled=True)  137 us
    all_gather x1, waiting for transfers between devices, proceed_stacks_all(): extra = all_gather(page, shard_axis)  51.3 us
    another operation x1, loops' own time, shards(): lax.scan(absorb_step, softmax_state, (stacked, jnp.arange(block_count, dt...  11 us
    reshape x1, local copies, waits for them, and re-layouts, shards(): stacked = kv_piece.reshape(block_count, block_rows, kv_piece.shape[1])  7.41 us
  transfers between devices with their start and end apart: 2, of which 2 were waited for; matrix products, arithmetic and copies ran while one was open for 0% of the time, Pallas kernels for 0%

profile of v1, /device:TPU:0, one launch (start us, length us, event | category | flops | bytes accessed | tf_op | source)
XLA Modules:
  0.0 246.7 jit_solution(16325013053625180314)
XLA Ops:
  6.5 0.0 copy-start
  6.5 0.0 all-gather.4.cloned.1.call-start
  6.5 1.5 constant_dynamic-update-slice_fusion.4
  8.0 0.2 copy-done.2
  8.2 0.1 constant_dynamic-update-slice_fusion.3
  8.3 0.2 copy-done.3
  8.5 0.1 constant_dynamic-update-slice_fusion.2
  8.6 0.9 copy-done.4
  9.5 0.1 constant_dynamic-update-slice_fusion.1
  9.6 0.6 copy-done.1
  10.2 0.1 constant_dynamic-update-slice_fusion
  10.3 1.1 copy-done.7
  11.4 1.8 fusion.24
  13.3 0.8 slice.34
  14.1 0.0 all-gather.4.cloned.1.call-update
  14.1 0.0 all-gather.6.cloned.1.call-start
  14.2 0.7 slice.27
  14.9 136.6 %all-gather.4.cloned.1.call-done = bf16[4096,1024]{0,1:T(8,128)(2,1)} async-done(((bf16[256,1024]{0,1:T(8,128)(2,1)}), bf16[4096,1024]{0,1:T(8,128)(2,1)}) %all-gather.4.cloned.1.call-update) | async-done | bytes 8388624 | tf_op jit(solution)/shard_map/all_gather | solution.py:79
  151.5 7.4 %copy.26 = bf16[128,8,8,512]{3,2,0,1:T(8,128)(2,1)} copy(bf16[128,8,8,512]{3,2,1,0:T(8,128)(2,1)} %bitcast.58) | data formatting | bytes 16777216 | tf_op jit(solution)/shard_map/reshape | solution.py:83
  159.0 21.9 %while.21 = (s32[]{:T(128)}, f32[4,256]{1,0:T(4,128)S(1)}, f32[4,256]{1,0:T(4,128)S(1)}, f32[4,256,128]{2,1,0:T(8,128)S(1)}, f32[4,256]{1,0:T(4,128)S(1)}, /*ind...) while((s32[]{:T(128)}, f32[4,256]{1,0:T(4,128)S(1)}, ...), condition=%wide.region_7.8_spmd.clone, body=%wide.region_0.7_spmd.clone.sunk | while | flops 416944896 | bytes 23601552 | solution.py:100
  159.1 0.6 dynamic_slice.13
  161.0 6.1 %conditional.3 = ((f32[4,256]{1,0:T(4,128)S(1)}, f32[4,256]{1,0:T(4,128)S(1)}, f32[4,256,128]{2,1,0:T(8,128)S(1)}, f32[4,256]{1,0:T(4,128)S(1)}, f32[4,256]{1,0:T(4,128)S(1)}, /*index=5*/f32[4,256,128]{2,1,0:T(8,128)S(1)})) conditional(s32[]{:T(128)} %convert_element_type.40, (f32[4,256]{1,0:T(4,128)S(1)}, f32[4,256]{1,0:T(4,128)S(1)}, ...), branch_computations={%region_1.1_spmd, %region_2.6_spmd} | conditional | flops 416944896 | bytes 23600196 | solution.py:91
  161.0 1.3 dynamic-slice_bitcast_fusion
  162.4 0.5 fusion.27
  162.9 0.1 broadcast_compare_fusion
  163.0 0.7 fusion.3
  163.8 1.0 fusion.7
  164.9 1.1 convolution_add_fusion
  166.0 1.1 convolution_add_fusion.1
  167.1 0.6 dynamic_slice.13
  169.1 0.6 dynamic_slice.13
  171.1 0.6 dynamic_slice.13
  173.0 0.6 dynamic_slice.13
  175.0 0.6 dynamic_slice.13
  177.0 0.6 dynamic_slice.13
  179.0 0.6 dynamic_slice.13
  180.9 0.0 copy-start.5
  180.9 0.0 copy-start.6
  181.0 1.0 copy.18
  182.0 0.2 copy.19
  182.2 0.0 copy-done.5
  182.2 1.2 multiply_reduce_fusion
  183.4 0.0 copy-done.6
  183.4 0.1 multiply_convert_fusion
  183.5 1.7 convolution_convert_fusion
  185.2 0.0 all-gather.6.cloned.1.call-update
  185.2 51.3 %all-gather.6.cloned.1.call-done = bf16[512,2048]{1,0:T(8,128)(2,1)} async-done(((bf16[256,2048]{1,0:T(8,128)(2,1)}), bf16[512,2048]{1,0:T(8,128)(2,1)}) %all-gather.6.cloned.1.call-update) | async-done | bytes 2097168 | tf_op jit(solution)/shard_map/all_gather | solution.py:13
  236.5 3.3 %reduce_sum.42 = bf16[256,2048]{1,0:T(8,128)(2,1)} reduce(bf16[2,256,2048]{2,1,0:T(8,128)(2,1)} %bitcast.61, bf16[]{:T(256)} %constant.46.clone.1), dimensions={0}, to_apply=%region_9.10 | reduce | flops 524288 | bytes 3145730 | tf_op jit(solution)/shard_map/reduce_sum | solution.py:14
  (40 shorter events, 0.4 us)
Async XLA Ops:
  6.5 177.0 %copy-start = (bf16[512,2048]{1,0:T(8,128)(2,1)S(1)}, bf16[512,2048]{1,0:T(8,128)(2,1)}, u32[]{:S(2)}) copy-start(bf16[512,2048]{1,0:T(8,128)(2,1)} %param.21) | copy-start | bytes 6291460
  6.5 1.7 copy-start.2
  6.5 145.0 %all-gather.4.cloned.1.call-start = ((), (), s32[]{:S(2)}) async-start(), calls=%async_computation | async-start | bytes 8912896 | tf_op jit(solution)/shard_map/all_gather | solution.py:79
  6.5 2.0 copy-start.3
  8.2 1.3 copy-start.4
  8.5 1.7 copy-start.1
  10.2 1.2 copy-start.7
  14.1 222.4 %all-gather.6.cloned.1.call-start = ((), (), s32[]{:S(2)}) async-start(), calls=%async_computation.1 | async-start | bytes 3145728 | tf_op jit(solution)/shard_map/all_gather | solution.py:13
  180.9 1.2 copy-start.5
  180.9 2.4 copy-start.6
Sparse Core Ops, SparseCore 0:
  14.3 137.1 all-gather.3
  185.4 51.1 all-gather.5
